TPU v7x, 32 devices: a whole 2x2x4 slice. The times are simulated.
32 devices in a mesh: ep: 8 (over z, y), tp: 4 (over x, core).
Axes of the slice: x: 2, y: 2, z: 4, core: 2. Of those that a mesh axis runs over, the one named last changes fastest.
Arguments:
- queries: bfloat16 [4096, 1024], P('ep', 'tp'), may hold values from -200 to 200
- keys: bfloat16 [4096, 256], P('ep', 'tp'), may hold values from -4 to 4
- values: bfloat16 [4096, 256], P('ep', 'tp'), may hold values from -4 to 4
- cum_gate: float32 [4096, 16], P(None, 'tp'), may hold values from -823 to 0, as said below
- out_weight: bfloat16 [1024, 2048], P('tp'), may hold values from -1.1953125 to 1.1953125
- moe_tokens: bfloat16 [4096, 2048], P(('ep', 'tp')), may hold values from -6 to 6
- norm_gain: float32 [2048], replicated, may hold values from 0.1 to 1.9
- routes: int32 [4096, 2], P('ep'), may hold values from 0 to 15, all different within a row; in each aligned block of 128 rows (0 to 127, 128 to 255, ...) at most 24 rows name the same one
- route_weight: float32 [4096, 2], P(('ep', 'tp')), may hold values from 0.25 to 2
- gate_weight: bfloat16 [16, 2048, 1024], P('ep', None, 'tp'), may hold values from -0.125 to 0.125
- up_weight: bfloat16 [16, 2048, 1024], P('ep', None, 'tp'), may hold values from -0.125 to 0.125
- down_weight: bfloat16 [16, 1024, 2048], P('ep', 'tp'), may hold values from -0.1875 to 0.1875
- shared_gate: bfloat16 [2048, 1024], P(None, 'tp'), may hold values from -0.125 to 0.125
- shared_up: bfloat16 [2048, 1024], P(None, 'tp'), may hold values from -0.125 to 0.125
- shared_down: bfloat16 [1024, 2048], P('tp'), may hold values from -0.1875 to 0.1875
Outputs:
- attn_out: bfloat16 [4096, 2048], P(('ep', 'tp'))
- moe_out: bfloat16 [4096, 2048], P(('ep', 'tp'))
Inputs may be any that keep to these rules, and one draw needn't show every extreme that they name: `cum_gate`: each head's values never rise along positions. `routes`: each row names 2 different experts; among the rows of one device no expert is named by more than 24 rows, and some device reaches 24.
All inputs are finite; a program needn't handle non-finite values.
Results may differ from a plain program's by a relative error of at most 0.012.
Values may be sent and summed in bfloat16 or wider, within the bound.
A program may use at most 128 MiB of HBM per device.

v0:
```python
import jax
import jax.numpy as jnp
from jax import lax
from jax.sharding import PartitionSpec as P

HEAD_SIZE = 64
EXP_DEV = 2
TOPK = 2


NEG_FILL = -1e30
EPSILON = 1e-06


def shards(
    queries,
    keys,
    values,
    cum_gate,
    out_weight,
    moe_tokens,
    norm_gain,
    routes,
    route_weight,
    gate_weight,
    up_weight,
    down_weight,
    shared_gate,
    shared_up,
    shared_down,
):
    ep_count = lax.axis_size("ep")
    tp_count = lax.axis_size("tp")
    ep_index = lax.axis_index("ep")
    tp_index = lax.axis_index("tp")
    query_rows = queries.shape[0]
    kv_local = keys.shape[1] // HEAD_SIZE
    head_local = queries.shape[1] // HEAD_SIZE
    group_size = head_local // kv_local
    score_scale = HEAD_SIZE ** (-0.5)
    first_row = ep_index * query_rows
    stacked = jnp.concatenate([keys, values], axis=1)
    count = queries.shape[0]
    gates = lax.dynamic_slice_in_dim(cum_gate, first_row, count, 0)
    grouped = queries.reshape(count, kv_local, group_size, HEAD_SIZE)
    bias = gates.T.reshape(kv_local, group_size, count, 1)
    positions = first_row + jnp.arange(count, dtype=jnp.int32)
    groups = ((grouped, bias, positions, first_row + count - 1),)

    def key_block(running, sub_block, offset, group):
        grouped, query_bias, query_pos, last_query = group
        sub_rows = sub_block.shape[0]
        key_part = sub_block[:, : kv_local * HEAD_SIZE].reshape(sub_rows, kv_local, HEAD_SIZE)
        value_part = sub_block[:, kv_local * HEAD_SIZE :].reshape(sub_rows, kv_local, HEAD_SIZE)
        key_gate = lax.dynamic_slice_in_dim(cum_gate, offset, sub_rows, 0)
        scores = (
            jnp.einsum("tkgd,skd->kgts", grouped, key_part, preferred_element_type=jnp.float32)
            * score_scale
        )
        scores = scores + query_bias - key_gate.T.reshape(kv_local, group_size, 1, sub_rows)
        key_pos = offset + jnp.arange(sub_rows, dtype=jnp.int32)
        causal = key_pos[None, :] <= query_pos[:, None]
        scores = jnp.where(causal, scores, NEG_FILL)
        row_max, row_total, weighted = running
        new_max = jnp.maximum(row_max, jnp.max(scores, axis=-1))
        weight = jnp.where(causal, jnp.exp(scores - new_max[..., None]), 0.0)
        shrink = jnp.exp(row_max - new_max)
        row_total = row_total * shrink + jnp.sum(weight, axis=-1)
        weighted = weighted * shrink[..., None] + jnp.einsum(
            "kgts,skd->kgtd",
            weight.astype(jnp.bfloat16),
            value_part,
            preferred_element_type=jnp.float32,
        )
        return (new_max, row_total, weighted)

    def empty_state(group):
        shape_three = (kv_local, group_size, group[0].shape[0])
        return (
            jnp.full(shape_three, NEG_FILL, jnp.float32),
            jnp.zeros(shape_three, jnp.float32),
            jnp.zeros(shape_three + (HEAD_SIZE,), jnp.float32),
        )

    initial = tuple((empty_state(group) for group in groups))
    arrived_kv = lax.all_gather(stacked, "ep", axis=0, tiled=True)
    total_rows = arrived_kv.shape[0]
    sub_rows = 512

    def visit_block(number, carried):
        sub_start = number * sub_rows
        sub_block = lax.dynamic_slice_in_dim(arrived_kv, sub_start, sub_rows, 0)
        updated = []
        for member, group in enumerate(groups):
            state = carried[member]
            updated.append(
                lax.cond(
                    sub_start <= group[3],
                    lambda: key_block(state, sub_block, sub_start, group),
                    lambda: state,
                )
            )
        return tuple(updated)

    states = lax.fori_loop(0, total_rows // sub_rows, visit_block, initial)
    row_max, row_total, weighted = states[0]
    count = weighted.shape[2]
    mixed_heads = (
        (weighted / row_total[..., None])
        .transpose(2, 0, 1, 3)
        .reshape(count, head_local * HEAD_SIZE)
        .astype(jnp.bfloat16)
    )
    mixer_part = jnp.dot(mixed_heads, out_weight, preferred_element_type=jnp.float32)
    mixer_sum = lax.psum_scatter(
        mixer_part.astype(jnp.bfloat16), "tp", scatter_dimension=0, tiled=True
    )
    token_rows = moe_tokens.shape[0]
    model_width = moe_tokens.shape[1]
    token_f32 = moe_tokens.astype(jnp.float32)
    normed = (
        token_f32
        * lax.rsqrt(jnp.mean(token_f32 * token_f32, axis=-1, keepdims=True) + EPSILON)
        * norm_gain
    ).astype(jnp.bfloat16)
    experts_all = EXP_DEV * ep_count
    capacity = max(2, 3 * token_rows * TOPK // (2 * experts_all))
    slot_count = EXP_DEV * capacity
    per_device = routes.reshape(tp_count, token_rows * TOPK)
    one_hot = (per_device[..., None] == jnp.arange(experts_all, dtype=jnp.int32)).astype(jnp.int32)
    slot_rank = jnp.sum(one_hot * jnp.cumsum(one_hot, axis=1), axis=-1) - 1
    target = per_device // EXP_DEV
    local_expert = per_device % EXP_DEV
    own_target = lax.dynamic_index_in_dim(target, tp_index, 0, keepdims=False)
    own_local = lax.dynamic_index_in_dim(local_expert, tp_index, 0, keepdims=False)
    own_rank = lax.dynamic_index_in_dim(slot_rank, tp_index, 0, keepdims=False)
    own_place = own_target * slot_count + own_local * capacity + own_rank
    choice_row = jnp.arange(token_rows * TOPK, dtype=jnp.int32) // TOPK
    blank_row = jnp.zeros((1, model_width), jnp.bfloat16)
    source = jnp.full((ep_count * slot_count,), token_rows, jnp.int32).at[own_place].set(choice_row)
    padded = jnp.concatenate([normed, blank_row], axis=0)
    outgoing = padded[source].reshape(ep_count, slot_count, model_width)
    received = lax.all_to_all(outgoing, "ep", split_axis=0, concat_axis=0, tiled=True)
    arrived, normed_group = (
        lax.all_gather(received, "tp", axis=1, tiled=True),
        lax.all_gather(normed, "tp", axis=0, tiled=True),
    )
    expert_rows = arrived.reshape(ep_count * tp_count, EXP_DEV, capacity, model_width)
    gate_act = jnp.einsum(
        "secd,edf->secf", expert_rows, gate_weight, preferred_element_type=jnp.float32
    )
    up_act = jnp.einsum(
        "secd,edf->secf", expert_rows, up_weight, preferred_element_type=jnp.float32
    )
    hidden = (jax.nn.silu(gate_act) * up_act).astype(jnp.bfloat16)
    expert_part = jnp.einsum(
        "secf,efd->secd", hidden, down_weight, preferred_element_type=jnp.float32
    ).reshape(ep_count, tp_count * slot_count, model_width)
    shared_hidden = (
        jax.nn.silu(jnp.dot(normed_group, shared_gate, preferred_element_type=jnp.float32))
        * jnp.dot(normed_group, shared_up, preferred_element_type=jnp.float32)
    ).astype(jnp.bfloat16)
    shared_part = jnp.dot(shared_hidden, shared_down, preferred_element_type=jnp.float32)
    expert_sum, shared_sum = (
        lax.psum_scatter(
            expert_part.astype(jnp.bfloat16), "tp", scatter_dimension=1, tiled=True
        ).astype(jnp.float32),
        lax.psum_scatter(
            shared_part.astype(jnp.bfloat16), "tp", scatter_dimension=0, tiled=True
        ).astype(jnp.float32),
    )
    returned = lax.all_to_all(
        expert_sum.astype(jnp.bfloat16), "ep", split_axis=0, concat_axis=0, tiled=True
    )
    picked = returned.reshape(ep_count * slot_count, model_width)[own_place].reshape(
        token_rows, TOPK, model_width
    )
    routed = jnp.sum(route_weight[..., None] * picked.astype(jnp.float32), axis=1)
    moe_out = (routed + shared_sum).astype(jnp.bfloat16)
    return (mixer_sum, moe_out)


def solution(mesh):
    in_specs = (
        P("ep", "tp"),
        P("ep", "tp"),
        P("ep", "tp"),
        P(None, "tp"),
        P("tp", None),
        P(("ep", "tp"), None),
        P(),
        P("ep", None),
        P(("ep", "tp"), None),
        P("ep", None, "tp"),
        P("ep", None, "tp"),
        P("ep", "tp", None),
        P(None, "tp"),
        P(None, "tp"),
        P("tp", None),
    )
    out_specs = (P(("ep", "tp"), None), P(("ep", "tp"), None))
    return jax.shard_map(shards, mesh=mesh, in_specs=in_specs, out_specs=out_specs, check_vma=False)
```

profile of v0, /device:TPU:0, one launch (start us, length us, event | category | flops | bytes accessed | tf_op | source)
XLA Modules:
  0.0 321.3 jit_solution(10754575705746269842)
XLA Ops:
  7.2 1.0 copy.25
  8.6 2.3 reduce-window.6
  11.2 1.4 scatter_custom_fusion
  12.7 1.2 fusion.44
  13.9 1.2 fusion.46
  15.2 3.1 gather_fusion
  18.4 44.6 %all_to_all.10 = bf16[8,48,2048]{2,1,0:T(8,128)(2,1)} all-to-all(bf16[8,48,2048]{2,1,0:T(8,128)(2,1)} %bitcast.140), channel_id=1, replica_groups=mesh['ep'=8,'tp'=4] {'ep'}, dimensions={0} | all-to-all | bytes 3145728 | tf_op jit(solution)/shard_map/all_to_all | solution.py:143
  63.0 0.7 all-gather.8.cloned.1.call-update
  63.8 0.7 pad_maximum_fusion
  64.5 44.0 %all-gather.6.cloned.1.call-done = bf16[8,192,2048]{2,1,0:T(8,128)(2,1)} async-done(((bf16[8,48,2048]{2,1,0:T(8,128)(2,1)}), bf16[8,192,2048]{2,1,0:T(8,128)(2,1)}) %all-gather.6.cloned.1.call-update) | async-done | bytes 6291472 | tf_op jit(solution)/shard_map/all_gather | solution.py:145
  108.5 6.4 %fusion.26 = f32[2,32,24,256]{3,2,1,0:T(8,128)} fusion(bf16[32,2,24,2048]{3,2,1,0:T(8,128)(2,1)} %bitcast.151, bf16[2,2048,256]{2,1,0:T(8,128)(2,1)} %param.28), kind=kOutput, calls=%fused_computation.35 | convolution fusion | flops 1610612736 | bytes 9961472 | tf_op jit(solution)/shard_map/secd,edf->secf/dot_general | solution.py:149
  114.9 10.7 %convert_bitcast_fusion = bf16[32,2,24,2048]{3,2,0,1:T(8,128)(2,1)} fusion(bf16[2,256,2048]{2,1,0:T(8,128)(2,1)S(1)} %copy-done, f32[2,32,24,256]{3,2,1,0:T(8,128)} %fusion.26, bf16[2,2048,256]{2,1,0:T(8,128)(2,1)} %param.29, bf16[32,2,24,2048]{3,2,1,0:T(8,128)(2,1)} %bitcast.152), kind=kOutput, calls=%fused_computation.32 | convolution fusion | flops 3226730496 | bytes 18350080 | tf_op jit(solution)/shard_map/secf,efd->secd/dot_general | solution.py:156
  125.6 6.6 %copy.31 = bf16[32,2,24,2048]{3,2,1,0:T(8,128)(2,1)} copy(bf16[32,2,24,2048]{3,2,0,1:T(8,128)(2,1)} %convert_bitcast_fusion) | data formatting | bytes 12582912 | tf_op jit(solution)/shard_map/convert_element_type | solution.py:166
  132.2 0.9 all-gather.8.cloned.1.call-done
  133.4 3.1 fusion.67
  136.5 6.0 %convolution_convert_fusion = bf16[512,2048]{1,0:T(8,128)(2,1)} fusion(bf16[256,2048]{1,0:T(8,128)(2,1)} %param.33, bf16[512,2048]{1,0:T(8,128)(2,1)} %all-gather.8.cloned.1.call-done, bf16[2048,256]{1,0:T(8,128)(2,1)} %param.32, f32[512,256]{1,0:T(8,128)} %fusion.67), kind=kOutput, calls=%fused_computation.37 | convolution fusion | flops 1075576832 | bytes 6815744 | tf_op jit(solution)/shard_map/dot_general | solution.py:163
  142.9 0.7 dynamic-slice_bitcast_fusion.5
  143.6 31.6 %all-gather.4.cloned.1.call-done = bf16[4096,128]{0,1:T(8,128)(2,1)} async-done(((bf16[512,128]{0,1:T(8,128)(2,1)}), bf16[4096,128]{0,1:T(8,128)(2,1)}) %all-gather.4.cloned.1.call-update) | async-done | bytes 1048592 | tf_op jit(solution)/shard_map/all_gather | solution.py:86
  175.3 11.4 %while.18 = (s32[]{:T(128)}, f32[1,4,512]{2,1,0:T(4,128)S(1)}, f32[1,4,512]{2,1,0:T(4,128)S(1)}, f32[1,4,512,64]{2,3,1,0:T(8,128)S(1)}, s32[]{:T(128)}, /*index=...) while((s32[]{:T(128)}, f32[1,4,512]{2,1,0:T(4,128)S(1)}, ...), condition=%wide.region_5.6_spmd.clone, body=%wide.region_0.5_spmd.clone.sunk | while | flops 288889856 | bytes 32059768 | solution.py:105
  175.3 11.0 %conditional.3 = ((f32[1,4,512]{2,1,0:T(4,128)S(1)}, f32[1,4,512]{2,1,0:T(4,128)S(1)}, f32[1,4,512,64]{2,3,1,0:T(8,128)S(1)})) conditional(s32[]{:T(128)} %convert_element_type.117, (f32[1,4,512]{2,1,0:T(4,128)S(1)}, f32[1,4,512]{2,1,0:T(4,128)S(1)}, f32[1,4,512,64]{2,3,1,0:T(8,128)S(1)}) %tuple.58, (s32[]{:T(128)}, s32[]{:T(128)}, ...), branch_computations={%region_1.0_spmd, %region_2.4_spmd} | conditional | flops 288889856 | bytes 32057474 | solution.py:97
  175.4 0.7 dynamic-slice_bitcast_fusion.4
  176.3 3.9 %fusion.6 = (f32[4,512]{1,0:T(4,128)S(1)}, f32[512,512,4]{1,0,2:T(8,128)}) fusion(f32[4,512]{1,0:T(4,128)S(1)} %dynamic-slice_bitcast_fusion.4, f32[4,512]{1,0:T(4,128)S(1)} %bitcast.145, pred[512,512]{0,1:T(8,128)(4,1)S(1)} %broadcast_compare_fusion, bf16[512,1,4,64]{0,3,2,1:T(8,128)(2,1)S(1)} %get-tuple-element.249, ...), kind=kOutput, calls=%fused_computation.10 | convolution fusion | flops 139458560 | bytes 4808708 | tf_op jit(solution)/shard_map/while/body/eval_jaxpr/cond/branch_1_fun/tkgd,skd->kgts/dot_general | solution.py:57
  180.3 4.1 %fusion.14 = f32[1,4,512,64]{2,3,1,0:T(8,128)S(1)} fusion(f32[512,512,4]{1,0,2:T(8,128)} %get-tuple-element.330, f32[4,512]{1,0:T(4,128)S(1)} %bitcast.141, f32[4,512]{1,0:T(4,128)S(1)} %dynamic-slice_bitcast_fusion.4, f32[4,512]{1,0:T(4,128)S(1)} %bitcast.146, pred[512,512]{0,1:T(8,128)(4,1)S(1)} %broadcast_compare_fusion, ...), kind=kOutput, calls=%fused_computation.15 | convolution fusion | flops 141819904 | bytes 5603336 | tf_op jit(solution)/shard_map/while/body/eval_jaxpr/cond/branch_1_fun/kgts,skd->kgtd/dot_general | solution.py:69
  184.8 1.5 fusion.5
  186.8 3.6 %convolution_convert_fusion.1 = bf16[512,2048]{1,0:T(8,128)(2,1)} fusion(bf16[512,256]{0,1:T(8,128)(2,1)S(1)} %bitcast.143, bf16[256,2048]{1,0:T(8,128)(2,1)} %param.23), kind=kOutput, calls=%fused_computation.38 | convolution fusion | flops 537919488 | bytes 3407872 | tf_op jit(solution)/shard_map/dot_general | solution.py:114
  190.4 45.1 %reduce-scatter.6.cloned.1.call-done = bf16[8,48,2048]{2,1,0:T(8,128)(2,1)} async-done(((bf16[8,192,2048]{2,1,0:T(8,128)(2,1)}), bf16[8,48,2048]{2,1,0:T(8,128)(2,1)}) %reduce-scatter.6.cloned.1.call-update) | async-done | bytes 1572880 | tf_op jit(solution)/shard_map/reduce_scatter | solution.py:165
  235.5 29.4 %all-to-all-start.1 = ((bf16[8,48,2048]{2,1,0:T(8,128)(2,1)}), bf16[8,48,2048]{2,1,0:T(8,128)(2,1)}, u32[]{:S(2)}, u32[]{:S(2)}) async-start(bf16[8,48,2048]{2,1,0:T(8,128)(2,1)} %reduce-scatter.6.cloned.1.call-done), calls=%async_computation.3 | async-start | bytes 3145728 | tf_op jit(solution)/shard_map/all_to_all | solution.py:172
  265.0 36.5 %all-to-all-done.1 = bf16[8,48,2048]{2,1,0:T(8,128)(2,1)} async-done(((bf16[8,48,2048]{2,1,0:T(8,128)(2,1)}), bf16[8,48,2048]{2,1,0:T(8,128)(2,1)}, u32[]{:S(2)}, u32[]{:S(2)}) %all-to-all-start.1) | async-done | bytes 1572896 | tf_op jit(solution)/shard_map/all_to_all | solution.py:172
  301.5 4.0 %gather_fusion.1 = bf16[256,2048]{1,0:T(8,128)(2,1)S(1)} fusion(bf16[384,2048]{1,0:T(8,128)(2,1)} %bitcast.35, s32[1024]{0:T(1024)S(1)} %pad_clamp_fusion), kind=kCustom, calls=%fused_computation.1 | custom fusion | bytes 2098176 | tf_op jit(solution)/shard_map/gather | solution.py:175
  305.5 2.3 reshape.162
  307.8 4.7 %multiply_reduce_fusion = f32[128,2048]{1,0:T(8,128)S(1)} fusion(f32[128,2,2048]{2,1,0:T(2,128)} %reshape.162, f32[128,2]{1,0:T(8,128)S(1)} %copy.24), kind=kLoop, calls=%fused_computation.42 | loop fusion | flops 786432 | bytes 3146752 | tf_op jit(solution)/shard_map/reduce_sum | solution.py:178
  312.6 1.9 add_convert_fusion
  (72 shorter events, 2.7 us)
Async XLA Ops:
  7.2 107.7 %copy-start = (bf16[2,256,2048]{2,1,0:T(8,128)(2,1)S(1)}, bf16[2,256,2048]{2,1,0:T(8,128)(2,1)}, u32[]{:S(2)}) copy-start(bf16[2,256,2048]{2,1,0:T(8,128)(2,1)} %param.30) | copy-start | bytes 6291460
  7.2 101.3 %all-gather.6.cloned.1.call-start = ((), (), s32[]{:S(2)}) async-start(), calls=%async_computation.7 | async-start | bytes 7864320 | tf_op jit(solution)/shard_map/all_gather | solution.py:145
  15.2 3.2 copy-start.2
  18.3 45.4 %copy-start.4 = (bf16[512,64]{0,1:T(8,128)(2,1)S(1)}, bf16[512,64]{0,1:T(8,128)(2,1)}, u32[]{:S(2)}) copy-start(bf16[512,64]{0,1:T(8,128)(2,1)} %param.21) | copy-start | bytes 196612
  18.4 45.4 %copy-start.5 = (bf16[512,64]{0,1:T(8,128)(2,1)S(1)}, bf16[512,64]{0,1:T(8,128)(2,1)}, u32[]{:S(2)}) copy-start(bf16[512,64]{0,1:T(8,128)(2,1)} %param.20) | copy-start | bytes 196612
  62.9 70.2 %all-gather.8.cloned.1.call-start = ((), (), s32[]{:S(2)}) async-start(), calls=%async_computation.9 | async-start | bytes 2621440 | tf_op jit(solution)/shard_map/all_gather | solution.py:146
  63.7 111.5 %all-gather.4.cloned.1.call-start = ((), (), s32[]{:S(2)}) async-start(), calls=%async_computation.5 | async-start | bytes 1179648 | tf_op jit(solution)/shard_map/all_gather | solution.py:86
  64.4 171.1 %reduce-scatter.6.cloned.1.call-start = ((), (), s32[]{:S(2)}) async-start(), calls=%async_computation.8 | async-start | bytes 7864320 | tf_op jit(solution)/shard_map/reduce_scatter | solution.py:165
  132.2 1.2 copy-start.7
  132.2 180.3 %reduce-scatter.8.cloned.1.call-start = ((), (), s32[]{:S(2)}) async-start(), calls=%async_computation.10 | async-start | bytes 2621440 | tf_op jit(solution)/shard_map/reduce_scatter | solution.py:168
  136.5 6.3 %copy-start.3 = (bf16[512,256]{1,0:T(8,128)(2,1)S(1)}, bf16[512,256]{1,0:T(8,128)(2,1)}, u32[]{:S(2)}) copy-start(bf16[512,256]{1,0:T(8,128)(2,1)} %param.19) | copy-start | bytes 786436
  142.5 172.0 %reduce-scatter.4.cloned.1.call-start = ((), (), s32[]{:S(2)}) async-start(), calls=%async_computation.6 | async-start | bytes 2621440 | tf_op jit(solution)/shard_map/reduce_scatter | solution.py:115
  180.2 4.5 %copy-start.1 = (f32[512,512,4]{1,0,2:T(8,128)S(1)}, f32[512,512,4]{1,0,2:T(8,128)}, u32[]{:S(2)}) copy-start(f32[512,512,4]{1,0,2:T(8,128)} %get-tuple-element.330) | copy-start | bytes 12582916 | tf_op jit(solution)/shard_map/while/body/eval_jaxpr/cond
  186.7 78.2 %copy-start.6 = (f32[128,2]{0,1:T(2,128)S(1)}, f32[128,2]{0,1:T(2,128)}, u32[]{:S(2)}) copy-start(f32[128,2]{0,1:T(2,128)} %param.27) | copy-start | bytes 3076
  235.5 66.0 %all-to-all-start.1 = ((bf16[8,48,2048]{2,1,0:T(8,128)(2,1)}), bf16[8,48,2048]{2,1,0:T(8,128)(2,1)}, u32[]{:S(2)}, u32[]{:S(2)}) async-start(bf16[8,48,2048]{2,1,0:T(8,128)(2,1)} %reduce-scatter.6.cloned.1.call-done), calls=%async_computation.3 | async-start | bytes 3145728 | tf_op jit(solution)/shard_map/all_to_all | solution.py:172
Sparse Core Ops, SparseCore 0:
  63.1 45.3 all-gather.5
  110.6 22.5 all-gather.7
  135.8 39.3 all-gather.3
  177.6 57.8 reduce-scatter.5
  237.9 31.1 reduce-scatter.7
  272.0 31.1 reduce-scatter.3
where the time goes:
time: 323 us; the launch traced here: 321 us
  waiting for transfers between devices  159 us (49%)
  blocking collectives  44.6 us (14%)
  matrix products  37.8 us (12%)
  starting transfers between devices  29.8 us (9%)
  local copies, waits for them, and re-layouts  21.4 us (7%)
  between operations  14.3 us (4%)
  other arithmetic  14.1 us (4%)
    reduce_scatter x1, waiting for transfers between devices, shards(): lax.psum_scatter(expert_part.astype(jnp.bfloat16), 'tp', scatter_dimensio...  45.1 us
    all_to_all x1, blocking collectives, shards(): lax.all_to_all(outgoing, 'ep', split_axis=0, concat_axis=0, tiled=True)  44.6 us
    all_gather x1, waiting for transfers between devices, shards(): lax.all_gather(received, 'tp', axis=1, tiled=True)  44 us
    all_to_all x1, waiting for transfers between devices, shards(): lax.all_to_all(expert_sum.astype(jnp.bfloat16), 'ep', split_axis=0, conca...  36.5 us
    all_gather x1, waiting for transfers between devices, shards(): arrived_kv = lax.all_gather(stacked, 'ep', axis=0, tiled=True)  31.6 us
    all_to_all x1, starting transfers between devices, shards(): lax.all_to_all(expert_sum.astype(jnp.bfloat16), 'ep', split_axis=0, conca...  29.4 us
    dot_general x1, matrix products, shards(): jnp.einsum('secf,efd->secd', hidden, down_weight, preferred_element_type=...  10.7 us
    convert_element_type x1, local copies, waits for them, and re-layouts, shards(): expert_part.astype(jnp.bfloat16)  6.58 us
  transfers between devices with their start and end apart: 7, of which 5 were waited for; matrix products, arithmetic and copies ran while one was open for 19% of the time, Pallas kernels for 0%

commit v1 on v0

v1 whole, which is shorter than its diff:
```python
import functools

import jax
import jax.numpy as jnp
from jax import lax
from jax.experimental import pallas as pl
from jax.experimental.pallas import tpu as pltpu
from jax.sharding import PartitionSpec as P

HEAD_SIZE = 64
EXP_DEV = 2
TOPK = 2


NEG_FILL = -1e30
EPSILON = 1e-06
LOG2E = 1.4426950408889634


def attend_kernel(heads, scale, block_ref, q_ref, kv_ref, bias_ref, out_ref, max_ref, acc_ref):
    rows = q_ref.shape[0]
    own = block_ref[0]
    max_ref[...] = jnp.full_like(max_ref, NEG_FILL)
    acc_ref[...] = jnp.zeros_like(acc_ref)

    def visit(block, diagonal):
        start = pl.multiple_of(block * rows, rows)
        keys = kv_ref[pl.ds(start, rows), :HEAD_SIZE]
        values = kv_ref[pl.ds(start, rows), HEAD_SIZE:]
        wide = jnp.concatenate([values, jnp.ones_like(values)], axis=1)
        for head in range(heads):
            query = q_ref[:, head * HEAD_SIZE : (head + 1) * HEAD_SIZE]
            scores = lax.dot_general(
                query, keys, (((1,), (1,)), ((), ())), preferred_element_type=jnp.float32
            )
            scores = scores * scale + bias_ref[head : head + 1, pl.ds(start, rows)]
            if diagonal:
                row_pos = lax.broadcasted_iota(jnp.int32, (rows, rows), 0)
                key_pos = lax.broadcasted_iota(jnp.int32, (rows, rows), 1)
                scores = jnp.where(key_pos <= row_pos, scores, NEG_FILL)
            old_max = max_ref[head, :, :1]
            new_max = jnp.maximum(old_max, jnp.max(scores, axis=1, keepdims=True))
            weight = jnp.exp2(scores - new_max).astype(jnp.bfloat16)
            part = jnp.dot(weight, wide, preferred_element_type=jnp.float32)
            acc_ref[head] = acc_ref[head] * jnp.exp2(old_max - new_max) + part
            max_ref[head] = jnp.broadcast_to(new_max, max_ref.shape[1:])

    def step(block, carry):
        visit(block, False)
        return carry

    visit(own, True)
    lax.fori_loop(0, own, step, 0)
    for head in range(heads):
        acc = acc_ref[head]
        out_ref[:, head * HEAD_SIZE : (head + 1) * HEAD_SIZE] = (
            acc[:, :HEAD_SIZE] / acc[:, HEAD_SIZE:]
        ).astype(out_ref.dtype)


def attention(queries, arrived_kv, cum_gate, ep_index):
    rows, width = queries.shape
    total = arrived_kv.shape[0]
    heads = width // HEAD_SIZE
    first = lax.dynamic_slice_in_dim(cum_gate, ep_index * rows, 1, 0)
    bias = ((first - cum_gate) * LOG2E).T
    return pl.pallas_call(
        functools.partial(attend_kernel, heads, HEAD_SIZE ** (-0.5) * LOG2E),
        out_shape=jax.ShapeDtypeStruct((rows, width), jnp.bfloat16),
        in_specs=[pl.BlockSpec(memory_space=pltpu.SMEM)]
        + [pl.BlockSpec(memory_space=pltpu.VMEM)] * 3,
        out_specs=pl.BlockSpec(memory_space=pltpu.VMEM),
        scratch_shapes=[
            pltpu.VMEM((heads, rows, 128), jnp.float32),
            pltpu.VMEM((heads, rows, 2 * HEAD_SIZE), jnp.float32),
        ],
        compiler_params=pltpu.CompilerParams(vmem_limit_bytes=32 * 1024 * 1024),
        cost_estimate=pl.CostEstimate(
            flops=4 * rows * total * width, bytes_accessed=total * 256, transcendentals=rows * total * heads
        ),
        name="attend",
    )(ep_index.reshape(1).astype(jnp.int32), queries, arrived_kv, bias)


def shards(
    queries,
    keys,
    values,
    cum_gate,
    out_weight,
    moe_tokens,
    norm_gain,
    routes,
    route_weight,
    gate_weight,
    up_weight,
    down_weight,
    shared_gate,
    shared_up,
    shared_down,
):
    ep_count = lax.axis_size("ep")
    tp_count = lax.axis_size("tp")
    ep_index = lax.axis_index("ep")
    tp_index = lax.axis_index("tp")
    arrived_kv = lax.all_gather(jnp.concatenate([keys, values], axis=1), "ep", axis=0, tiled=True)
    token_rows = moe_tokens.shape[0]
    model_width = moe_tokens.shape[1]
    token_f32 = moe_tokens.astype(jnp.float32)
    normed = (
        token_f32
        * lax.rsqrt(jnp.mean(token_f32 * token_f32, axis=-1, keepdims=True) + EPSILON)
        * norm_gain
    ).astype(jnp.bfloat16)
    experts_all = EXP_DEV * ep_count
    capacity = max(2, 3 * token_rows * TOPK // (2 * experts_all))
    slot_count = EXP_DEV * capacity
    per_device = routes.reshape(tp_count, token_rows * TOPK)
    one_hot = (per_device[..., None] == jnp.arange(experts_all, dtype=jnp.int32)).astype(jnp.int32)
    slot_rank = jnp.sum(one_hot * jnp.cumsum(one_hot, axis=1), axis=-1) - 1
    target = per_device // EXP_DEV
    local_expert = per_device % EXP_DEV
    own_target = lax.dynamic_index_in_dim(target, tp_index, 0, keepdims=False)
    own_local = lax.dynamic_index_in_dim(local_expert, tp_index, 0, keepdims=False)
    own_rank = lax.dynamic_index_in_dim(slot_rank, tp_index, 0, keepdims=False)
    own_place = own_target * slot_count + own_local * capacity + own_rank
    choice_row = jnp.arange(token_rows * TOPK, dtype=jnp.int32) // TOPK
    blank_row = jnp.zeros((1, model_width), jnp.bfloat16)
    source = jnp.full((ep_count * slot_count,), token_rows, jnp.int32).at[own_place].set(choice_row)
    padded = jnp.concatenate([normed, blank_row], axis=0)
    outgoing = padded[source].reshape(ep_count, slot_count, model_width)
    received = lax.all_to_all(outgoing, "ep", split_axis=0, concat_axis=0, tiled=True)
    received, arrived_kv = lax.optimization_barrier((received, arrived_kv))
    arrived = lax.all_gather(received, "tp", axis=1, tiled=True)
    mixed_heads = attention(queries, arrived_kv, cum_gate, ep_index)
    mixer_part = jnp.dot(mixed_heads, out_weight, preferred_element_type=jnp.float32).astype(
        jnp.bfloat16
    )
    arrived, mixer_part, normed_late = lax.optimization_barrier((arrived, mixer_part, normed))
    normed_group = lax.all_gather(normed_late, "tp", axis=0, tiled=True)
    expert_rows = arrived.reshape(ep_count * tp_count, EXP_DEV, capacity, model_width)
    gate_act = jnp.einsum(
        "secd,edf->secf", expert_rows, gate_weight, preferred_element_type=jnp.float32
    )
    up_act = jnp.einsum(
        "secd,edf->secf", expert_rows, up_weight, preferred_element_type=jnp.float32
    )
    hidden = (jax.nn.silu(gate_act) * up_act).astype(jnp.bfloat16)
    expert_part = jnp.einsum(
        "secf,efd->secd", hidden, down_weight, preferred_element_type=jnp.float32
    ).reshape(ep_count, tp_count * slot_count, model_width)
    expert_part, normed_group = lax.optimization_barrier(
        (expert_part.astype(jnp.bfloat16), normed_group)
    )
    expert_sum = lax.psum_scatter(expert_part, "tp", scatter_dimension=1, tiled=True)
    shared_hidden = (
        jax.nn.silu(jnp.dot(normed_group, shared_gate, preferred_element_type=jnp.float32))
        * jnp.dot(normed_group, shared_up, preferred_element_type=jnp.float32)
    ).astype(jnp.bfloat16)
    shared_part = jnp.dot(shared_hidden, shared_down, preferred_element_type=jnp.float32).astype(
        jnp.bfloat16
    )
    both_part = jnp.concatenate([mixer_part, shared_part], axis=1)
    expert_sum, both_part = lax.optimization_barrier((expert_sum, both_part))
    both_sum = lax.psum_scatter(both_part, "tp", scatter_dimension=0, tiled=True)
    mixer_sum = both_sum[:, :model_width]
    shared_sum = both_sum[:, model_width:].astype(jnp.float32)
    returned = lax.all_to_all(expert_sum, "ep", split_axis=0, concat_axis=0, tiled=True)
    picked = returned.reshape(ep_count * slot_count, model_width)[own_place].reshape(
        token_rows, TOPK, model_width
    )
    routed = jnp.sum(route_weight[..., None] * picked.astype(jnp.float32), axis=1)
    moe_out = (routed + shared_sum).astype(jnp.bfloat16)
    return (mixer_sum, moe_out)


def solution(mesh):
    in_specs = (
        P("ep", "tp"),
        P("ep", "tp"),
        P("ep", "tp"),
        P(None, "tp"),
        P("tp", None),
        P(("ep", "tp"), None),
        P(),
        P("ep", None),
        P(("ep", "tp"), None),
        P("ep", None, "tp"),
        P("ep", None, "tp"),
        P("ep", "tp", None),
        P(None, "tp"),
        P(None, "tp"),
        P("tp", None),
    )
    out_specs = (P(("ep", "tp"), None), P(("ep", "tp"), None))
    return jax.shard_map(shards, mesh=mesh, in_specs=in_specs, out_specs=out_specs, check_vma=False)
```

time: 323 us -> 277 us (0.86)
  blocking collectives: 44.6 us -> 0 us
  starting transfers between devices: 29.8 us -> 13.4 us
  waiting for transfers between devices: 159 us -> 174 us
  matrix products: 37.8 us -> 28.3 us
  other arithmetic: 14.1 us -> 18.7 us
  Pallas kernels: 0 us -> 3.83 us
    all_to_all x1 -> x0, blocking collectives: 44.6 us -> none  [shards(): lax.all_to_all(outgoing, 'ep', split_axis=0, concat_axis=0, tiled=True)]
    all_to_all x1 -> x2, starting transfers between devices: 29.4 us -> 13 us  [the longest x1 7.45 us: shards(): lax.all_to_all(outgoing, 'ep', split_axis=0, concat_axis=0, tiled=True)]
    all_gather x3, waiting for transfers between devices: 76.5 us -> 92.3 us  [the longest x1 52.4 us: shards(): lax.all_gather(jnp.concatenate([keys, values], axis=1), 'ep', axis=0, til...]
    dot_general x2 -> x0, matrix products: 7.99 us -> none  [the longest x1 4.06 us: key_block(): jnp.einsum('kgts,skd->kgtd', weight.astype(jnp.bfloat16), value_part, pre...]
    concatenate x1 -> x2, other arithmetic: 0.67 us -> 7.03 us  [the longest x1 6.26 us: shards(): both_part = jnp.concatenate([mixer_part, shared_part], axis=1)]
    pallas_call x0 -> x1, Pallas kernels: none -> 3.83 us  [attention(): pl.pallas_call(functools.partial(attend_kernel, heads, HEAD_SIZE ** (-0.5...]
    reduce_scatter x3 -> x2, waiting for transfers between devices: 45.2 us -> 44.8 us  [the longest x1 44.7 us: shards(): lax.psum_scatter(expert_part, 'tp', scatter_dimension=1, tiled=True)]
    all_to_all x1 -> x2, waiting for transfers between devices: 36.5 us -> 36.8 us  [the longest x1 36.8 us: shards(): lax.all_to_all(expert_sum, 'ep', split_axis=0, concat_axis=0, tiled=True)]
  transfers between devices with their start and end apart: 7 -> 7, of which waited for: 5 -> 5; matrix products, arithmetic and copies ran while one was open for 19% -> 19% of each run, Pallas kernels for 0% -> 1%
where the time goes in v1:
time: 277 us; the launch traced here: 276 us
  waiting for transfers between devices  174 us (63%)
  matrix products  28.3 us (10%)
  local copies, waits for them, and re-layouts  23.8 us (9%)
  other arithmetic  18.7 us (7%)
  between operations  14 us (5%)
  starting transfers between devices  13.4 us (5%)
  Pallas kernels  3.83 us (1%)
    all_gather x1, waiting for transfers between devices, shards(): lax.all_gather(jnp.concatenate([keys, values], axis=1), 'ep', axis=0, til...  52.4 us
    reduce_scatter x1, waiting for transfers between devices, shards(): lax.psum_scatter(expert_part, 'tp', scatter_dimension=1, tiled=True)  44.7 us
    all_gather x1, waiting for transfers between devices, shards(): arrived = lax.all_gather(received, 'tp', axis=1, tiled=True)  39.2 us
    all_to_all x1, waiting for transfers between devices, shards(): lax.all_to_all(expert_sum, 'ep', split_axis=0, concat_axis=0, tiled=True)  36.8 us
    dot_general x1, matrix products, shards(): jnp.einsum('secf,efd->secd', hidden, down_weight, preferred_element_type=...  10.8 us
    all_to_all x1, starting transfers between devices, shards(): lax.all_to_all(outgoing, 'ep', split_axis=0, concat_axis=0, tiled=True)  7.45 us
    convert_element_type x1, local copies, waits for them, and re-layouts, shards(): expert_part.astype(jnp.bfloat16)  6.58 us
    dot_general x1, matrix products, shards(): jnp.einsum('secd,edf->secf', expert_rows, gate_weight, preferred_element_...  6.39 us
  transfers between devices with their start and end apart: 7, of which 5 were waited for; matrix products, arithmetic and copies ran while one was open for 19% of the time, Pallas kernels for 1%

profile of v1, /device:TPU:0, one launch (start us, length us, event | category | flops | bytes accessed | tf_op | source)
XLA Modules:
  0.0 276.0 jit_solution(3750675223159940862)
XLA Ops:
  7.2 1.0 copy.22
  8.3 0.2 eq.28
  8.5 2.3 reduce-window.6
  11.2 1.4 scatter_custom_fusion
  12.6 1.2 fusion.20
  13.9 1.2 fusion.22
  15.2 3.1 %gather_fusion = bf16[384,2048]{1,0:T(8,128)(2,1)} fusion(bf16[129,2048]{1,0:T(8,128)(2,1)S(1)} %concatenate.9, s32[1024]{0:T(1024)S(1)} %pad_clamp_fusion.1), kind=kCustom, calls=%fused_computation | custom fusion | bytes 3147264 | tf_op jit(solution)/shard_map/gather | solution.py:131
  18.3 7.5 %all-to-all-start = ((bf16[8,48,2048]{2,1,0:T(8,128)(2,1)}), bf16[8,48,2048]{2,1,0:T(8,128)(2,1)}, u32[]{:S(2)}, u32[]{:S(2)}) async-start(bf16[8,48,2048]{2,1,0:T(8,128)(2,1)} %bitcast.78), calls=%async_computation | async-start | bytes 3145728 | tf_op jit(solution)/shard_map/all_to_all | solution.py:132
  26.1 0.8 pad_maximum_fusion.1
  27.0 52.4 %all-gather.4.cloned.1.call-done.kv_ref = bf16[4096,128]{1,0:T(8,128)(2,1)} async-done(((bf16[512,128]{1,0:T(8,128)(2,1)}), bf16[4096,128]{1,0:T(8,128)(2,1)}) %all-gather.4.cloned.1.call-update) | async-done | bytes 1048592 | tf_op jit(solution)/shard_map/all_gather | solution.py:106
  79.4 0.2 dynamic-slice_reduce_fusion
  79.7 1.2 copy-done.1
  80.9 3.8 %attend.1 = bf16[512,256]{1,0:T(8,128)(2,1)S(1)} custom-call(s32[1]{0:T(128)} %bitcast.5.block_ref, bf16[512,256]{1,0:T(8,128)(2,1)S(1)} %copy-done.2, bf16[4096,128]{1,0:T(8,128)(2,1)S(1)} %copy-done.1, f32[4,4096]{1,0:T(4,128)S(1)} %multiply_bitcast_fusion.bias_ref), custom_call_target="tpu_custom_call" | custom-call | flops 2147483648 | bytes 1048576 | tf_op jit(solution)/shard_map/attend/pallas_call | solution.py:67
  84.8 2.1 convolution_convert_fusion.1
  86.8 39.2 %all-gather.6.cloned.1.call-done = bf16[8,192,2048]{2,1,0:T(8,128)(2,1)} async-done(((bf16[8,48,2048]{2,1,0:T(8,128)(2,1)}), bf16[8,192,2048]{2,1,0:T(8,128)(2,1)}) %all-gather.6.cloned.1.call-update) | async-done | bytes 6291472 | tf_op jit(solution)/shard_map/all_gather | solution.py:134
  126.1 0.2 reduce-scatter.3.cloned.1.call-start
  126.3 6.4 %fusion.2 = f32[2,32,24,256]{3,2,1,0:T(8,128)} fusion(bf16[32,2,24,2048]{3,2,1,0:T(8,128)(2,1)} %bitcast.81, bf16[2,2048,256]{2,1,0:T(8,128)(2,1)} %param.24), kind=kOutput, calls=%fused_computation.6 | convolution fusion | flops 1610612736 | bytes 9961472 | tf_op jit(solution)/shard_map/secd,edf->secf/dot_general | solution.py:142
  132.7 10.8 %convert_bitcast_fusion = bf16[32,2,24,2048]{3,2,0,1:T(8,128)(2,1)} fusion(bf16[2,256,2048]{2,1,0:T(8,128)(2,1)S(1)} %copy-done, f32[2,32,24,256]{3,2,1,0:T(8,128)} %fusion.2, bf16[2,2048,256]{2,1,0:T(8,128)(2,1)} %param.25, bf16[32,2,24,2048]{3,2,1,0:T(8,128)(2,1)} %bitcast.82), kind=kOutput, calls=%fused_computation.3 | convolution fusion | flops 3226730496 | bytes 18350080 | tf_op jit(solution)/shard_map/secf,efd->secd/dot_general | solution.py:149
  143.5 6.6 %copy.30 = bf16[32,2,24,2048]{3,2,1,0:T(8,128)(2,1)} copy(bf16[32,2,24,2048]{3,2,0,1:T(8,128)(2,1)} %convert_bitcast_fusion) | data formatting | bytes 12582912 | tf_op jit(solution)/shard_map/convert_element_type | solution.py:153
  150.1 0.7 all-gather.8.cloned.1.call-done
  150.9 1.2 copy-done.9
  152.0 3.1 %fusion.43 = f32[512,256]{1,0:T(8,128)} fusion(bf16[512,2048]{1,0:T(8,128)(2,1)} %all-gather.8.cloned.1.call-done, bf16[2048,256]{1,0:T(8,128)(2,1)S(1)} %copy-done.9), kind=kOutput, calls=%fused_computation.78 | convolution fusion | flops 536870912 | bytes 3670016 | tf_op jit(solution)/shard_map/dot_general | solution.py:157
  155.1 5.9 %convolution_convert_fusion = bf16[512,2048]{1,0:T(8,128)(2,1)} fusion(bf16[256,2048]{1,0:T(8,128)(2,1)} %param.29, bf16[512,2048]{1,0:T(8,128)(2,1)} %all-gather.8.cloned.1.call-done, bf16[2048,256]{1,0:T(8,128)(2,1)} %param.28, f32[512,256]{1,0:T(8,128)} %fusion.43), kind=kOutput, calls=%fused_computation.9 | convolution fusion | flops 1075576832 | bytes 6815744 | tf_op jit(solution)/shard_map/dot_general | solution.py:160
  161.0 6.3 %pad_maximum_fusion = bf16[512,4096]{1,0:T(8,128)(2,1)} fusion(bf16[512,2048]{1,0:T(8,128)(2,1)} %convolution_convert_fusion, bf16[512,2048]{1,0:T(8,128)(2,1)} %convolution_convert_fusion.1), kind=kLoop, calls=%fused_computation.8 | loop fusion | flops 8388608 | bytes 8388608 | tf_op jit(solution)/shard_map/concatenate | solution.py:163
  167.3 44.7 %reduce-scatter.3.cloned.1.call-done = bf16[8,48,2048]{2,1,0:T(8,128)(2,1)} async-done(((bf16[8,192,2048]{2,1,0:T(8,128)(2,1)}), bf16[8,48,2048]{2,1,0:T(8,128)(2,1)}) %reduce-scatter.3.cloned.1.call-update) | async-done | bytes 1572880 | tf_op jit(solution)/shard_map/reduce_scatter | solution.py:155
  212.1 5.5 %all-to-all-start.1 = ((bf16[8,48,2048]{2,1,0:T(8,128)(2,1)}), bf16[8,48,2048]{2,1,0:T(8,128)(2,1)}, u32[]{:S(2)}, u32[]{:S(2)}) async-start(bf16[8,48,2048]{2,1,0:T(8,128)(2,1)} %reduce-scatter.3.cloned.1.call-done), calls=%async_computation.3 | async-start | bytes 3145728 | tf_op jit(solution)/shard_map/all_to_all | solution.py:168
  217.7 36.8 %all-to-all-done.1 = bf16[8,48,2048]{2,1,0:T(8,128)(2,1)} async-done(((bf16[8,48,2048]{2,1,0:T(8,128)(2,1)}), bf16[8,48,2048]{2,1,0:T(8,128)(2,1)}, u32[]{:S(2)}, u32[]{:S(2)}) %all-to-all-start.1) | async-done | bytes 1572896 | tf_op jit(solution)/shard_map/all_to_all | solution.py:168
  254.6 4.0 %gather_fusion.1 = bf16[256,2048]{1,0:T(8,128)(2,1)S(1)} fusion(bf16[384,2048]{1,0:T(8,128)(2,1)} %bitcast.18, s32[1024]{0:T(1024)S(1)} %pad_clamp_fusion), kind=kCustom, calls=%fused_computation.1 | custom fusion | bytes 2098176 | tf_op jit(solution)/shard_map/gather | solution.py:169
  258.5 2.3 reshape.100
  260.9 4.7 %multiply_reduce_fusion = f32[128,2048]{1,0:T(8,128)S(1)} fusion(f32[128,2,2048]{2,1,0:T(2,128)} %reshape.100, f32[128,2]{1,0:T(8,128)S(1)} %copy.31), kind=kLoop, calls=%fused_computation.14 | loop fusion | flops 786432 | bytes 3146752 | tf_op jit(solution)/shard_map/reduce_sum | solution.py:172
  265.6 1.9 slice.22
  267.5 1.9 add_convert_fusion
  (49 shorter events, 1.4 us)
Async XLA Ops:
  7.2 125.5 %copy-start = (bf16[2,256,2048]{2,1,0:T(8,128)(2,1)S(1)}, bf16[2,256,2048]{2,1,0:T(8,128)(2,1)}, u32[]{:S(2)}) copy-start(bf16[2,256,2048]{2,1,0:T(8,128)(2,1)} %param.26) | copy-start | bytes 6291460
  15.1 3.2 %copy-start.3 = (bf16[128,2048]{1,0:T(8,128)(2,1)}, bf16[128,2048]{1,0:T(8,128)(2,1)S(1)}, u32[]{:S(2)}) copy-start(bf16[128,2048]{1,0:T(8,128)(2,1)S(1)} %fusion.22) | copy-start | bytes 1572868
  18.3 7.5 %copy-start.6 = (bf16[512,64]{0,1:T(8,128)(2,1)S(1)}, bf16[512,64]{0,1:T(8,128)(2,1)}, u32[]{:S(2)}) copy-start(bf16[512,64]{0,1:T(8,128)(2,1)} %param.16) | copy-start | bytes 196612
  18.3 7.7 %copy-start.7 = (bf16[512,64]{0,1:T(8,128)(2,1)S(1)}, bf16[512,64]{0,1:T(8,128)(2,1)}, u32[]{:S(2)}) copy-start(bf16[512,64]{0,1:T(8,128)(2,1)} %param.17) | copy-start | bytes 196612
  18.3 61.1 %copy-start.5 = (f32[4096,4]{0,1:T(4,128)S(1)}, f32[4096,4]{0,1:T(4,128)}, u32[]{:S(2)}) copy-start(f32[4096,4]{0,1:T(4,128)} %param.18) | copy-start | bytes 196612
  18.3 61.0 %all-to-all-start = ((bf16[8,48,2048]{2,1,0:T(8,128)(2,1)}), bf16[8,48,2048]{2,1,0:T(8,128)(2,1)}, u32[]{:S(2)}, u32[]{:S(2)}) async-start(bf16[8,48,2048]{2,1,0:T(8,128)(2,1)} %bitcast.78), calls=%async_computation | async-start | bytes 3145728 | tf_op jit(solution)/shard_map/all_to_all | solution.py:132
  25.8 53.9 %copy-start.2 = (bf16[512,256]{1,0:T(8,128)(2,1)S(1)}, bf16[512,256]{1,0:T(8,128)(2,1)}, u32[]{:S(2)}) copy-start(bf16[512,256]{1,0:T(8,128)(2,1)} %q_ref.1) | copy-start | bytes 786436
  25.8 53.5 %all-gather.4.cloned.1.call-start = ((), (), s32[]{:S(2)}) async-start(), calls=%async_computation.4 | async-start | bytes 1179648 | tf_op jit(solution)/shard_map/all_gather | solution.py:106
  26.9 99.1 %all-gather.6.cloned.1.call-start = ((), (), s32[]{:S(2)}) async-start(), calls=%async_computation.5 | async-start | bytes 7864320 | tf_op jit(solution)/shard_map/all_gather | solution.py:134
  79.4 71.4 %all-gather.8.cloned.1.call-start = ((), (), s32[]{:S(2)}) async-start(), calls=%async_computation.6 | async-start | bytes 2621440 | tf_op jit(solution)/shard_map/all_gather | solution.py:140
  79.7 1.2 copy-start.1
  80.9 3.8 %copy-start.4 = (bf16[256,2048]{1,0:T(8,128)(2,1)S(1)}, bf16[256,2048]{1,0:T(8,128)(2,1)}, u32[]{:S(2)}) copy-start(bf16[256,2048]{1,0:T(8,128)(2,1)} %param.19) | copy-start | bytes 3145732
  126.1 86.0 %reduce-scatter.3.cloned.1.call-start = ((), (), s32[]{:S(2)}) async-start(), calls=%async_computation.7 | async-start | bytes 7864320 | tf_op jit(solution)/shard_map/reduce_scatter | solution.py:155
  150.8 1.2 copy-start.9
  150.8 114.8 %reduce-scatter.5.cloned.1.call-start = ((), (), s32[]{:S(2)}) async-start(), calls=%async_computation.8 | async-start | bytes 5242880 | tf_op jit(solution)/shard_map/reduce_scatter | solution.py:165
  212.1 5.5 %copy-start.8 = (f32[128,2]{0,1:T(2,128)S(1)}, f32[128,2]{0,1:T(2,128)}, u32[]{:S(2)}) copy-start(f32[128,2]{0,1:T(2,128)} %param.23) | copy-start | bytes 3076
  212.1 42.5 %all-to-all-start.1 = ((bf16[8,48,2048]{2,1,0:T(8,128)(2,1)}), bf16[8,48,2048]{2,1,0:T(8,128)(2,1)}, u32[]{:S(2)}, u32[]{:S(2)}) async-start(bf16[8,48,2048]{2,1,0:T(8,128)(2,1)} %reduce-scatter.3.cloned.1.call-done), calls=%async_computation.3 | async-start | bytes 3145728 | tf_op jit(solution)/shard_map/all_to_all | solution.py:168
Sparse Core Ops, SparseCore 0:
  29.3 49.9 all-gather.3
  80.9 45.1 all-gather.5
  128.2 22.5 all-gather.7
  153.2 58.8 reduce-scatter.2
  214.4 44.5 reduce-scatter.4
